TPU v7x, 32 devices: a whole 2x2x4 slice. The times are simulated.
32 devices in a mesh: sp: 8 (over z, y), tp: 4 (over x, core).
Axes of the slice: x: 2, y: 2, z: 4, core: 2. Of those that a mesh axis runs over, the one named last changes fastest.
Arguments:
- tokens: bfloat16 [3072, 2048], P('sp', 'tp'), may hold values from -6 to 6
- norm_gain: float32 [3, 2048], replicated, may hold values from 0.1 to 1.9
- w_value: bfloat16 [3, 2048, 1024], P(None, 'sp', 'tp'), may hold values from -0.125 to 0.125
- w_gate: bfloat16 [3, 2048, 1024], P(None, 'sp', 'tp'), may hold values from -0.125 to 0.125
- conv_taps: float32 [3, 31, 1024], P(None, None, 'tp'), may hold values from -2.4 to 2.4
- conv_bias: float32 [3, 1024], P(None, 'tp'), may hold values from -3 to 3
- ln_gain: float32 [3, 1024], P(None, 'tp'), may hold values from 0.1 to 1.9
- ln_shift: float32 [3, 1024], P(None, 'tp'), may hold values from -3 to 3
- w_out: bfloat16 [3, 1024, 2048], P(None, 'tp', 'sp'), may hold values from -0.1875 to 0.1875
Outputs:
- stream: bfloat16 [3072, 2048], P('sp', 'tp')
All inputs are finite; a program needn't handle non-finite values.
Results may differ from a plain program's by a relative error of at most 0.015.
Values may be sent and summed in bfloat16 or wider, within the bound.
A program may use at most 64 MiB of HBM per device.

v0:
```python
import jax
import jax.numpy as jnp
from jax import lax
from jax.sharding import PartitionSpec as P

norm_floor = 0.01


def with_halo(array, sides, width):
    for axis, dim in sides:
        size, length = (lax.axis_size(axis), array.shape[dim])
        up = [(i, (i + 1) % size) for i in range(size - 1)]
        down = [(j, i) for i, j in up]
        last = lax.slice_in_dim(array, length - width, length, axis=dim)
        first = lax.slice_in_dim(array, 0, width, axis=dim)
        before = lax.ppermute(last, axis, up)
        after = lax.ppermute(first, axis, down)
        array = jnp.concatenate([before, array, after], axis=dim)
    return array


def body(tokens, norm_gain, w_value, w_gate, conv_taps, conv_bias, ln_gain, ln_shift, w_out):
    stream = tokens
    layer_count = w_value.shape[0]
    reach = conv_taps.shape[1] // 2
    local_channels = w_value.shape[2]
    channels = local_channels * lax.axis_size("tp")
    tok_rows = tokens.shape[0]
    whole_value, whole_gate = (
        lax.all_gather(w_value, "sp", axis=1, tiled=True),
        lax.all_gather(w_gate, "sp", axis=1, tiled=True),
    )
    whole_out = lax.all_gather(w_out, "sp", axis=2, tiled=True)
    for layer_index in range(layer_count):
        whole_rows = lax.all_gather(stream, "tp", axis=1, tiled=True)
        rows_f32 = whole_rows.astype(jnp.float32)
        scale_rows = lax.rsqrt(jnp.mean(rows_f32 * rows_f32, axis=-1, keepdims=True) + norm_floor)
        normed = (rows_f32 * scale_rows * norm_gain[layer_index]).astype(jnp.bfloat16)
        value_rows = jnp.dot(normed, whole_value[layer_index], preferred_element_type=jnp.float32)
        gate_rows = jnp.dot(normed, whole_gate[layer_index], preferred_element_type=jnp.float32)
        gated_input = (value_rows * jax.nn.sigmoid(gate_rows)).astype(jnp.bfloat16)
        padded = with_halo(gated_input, (("sp", 0),), reach)
        padded = padded.astype(jnp.float32)
        convolved = jnp.zeros((tok_rows, local_channels), jnp.float32) + conv_bias[layer_index]
        for offset in range(2 * reach + 1):
            convolved = (
                convolved + conv_taps[layer_index, offset] * padded[offset : offset + tok_rows]
            )
        moments = lax.psum(
            (
                jnp.sum(convolved, axis=-1, keepdims=True),
                jnp.sum(convolved * convolved, axis=-1, keepdims=True),
            ),
            "tp",
        )
        average = moments[0] / channels
        spread = moments[1] / channels - average * average
        activated = jax.nn.silu(
            (convolved - average) * lax.rsqrt(spread + norm_floor) * ln_gain[layer_index]
            + ln_shift[layer_index]
        ).astype(jnp.bfloat16)
        partial_rows = jnp.dot(
            activated, whole_out[layer_index], preferred_element_type=jnp.float32
        )
        summed = lax.psum_scatter(
            partial_rows.astype(jnp.bfloat16), "tp", scatter_dimension=1, tiled=True
        ).astype(jnp.float32)
        stream = (stream.astype(jnp.float32) + summed).astype(jnp.bfloat16)
    return stream


def solution(mesh):
    placed = (
        P("sp", "tp"),
        P(),
        P(None, "sp", "tp"),
        P(None, "sp", "tp"),
        P(None, None, "tp"),
        P(None, "tp"),
        P(None, "tp"),
        P(None, "tp"),
        P(None, "tp", "sp"),
    )
    return jax.shard_map(body, mesh=mesh, in_specs=placed, out_specs=P("sp", "tp"), check_vma=False)
```

profile of v0, /device:TPU:0, one launch (start us, length us, event | category | flops | bytes accessed | tf_op | source)
XLA Modules:
  0.0 407.2 jit_solution(14767884248414049821)
XLA Ops:
  6.5 0.7 all-gather.7.cloned.1.call-update
  7.3 0.0 all-gather.11.cloned.1.call-start
  7.3 0.7 all-gather.11.cloned.1.call-update
  8.0 0.0 all-gather.9.cloned.1.call-start
  8.1 0.7 all-gather.9.cloned.1.call-update
  8.7 0.0 all-gather.13.cloned.1.call-start
  8.8 0.5 all-gather.13.cloned.1.call-update
  9.3 0.0 reduce-scatter.4.cloned.1.call-start
  9.4 0.8 fusion.155
  10.2 0.8 fusion.153
  11.0 1.0 fusion.151
  12.0 1.1 fusion.150
  13.0 0.9 fusion.152
  13.9 17.3 %all-gather.7.cloned.1.call-done = bf16[384,2048]{1,0:T(8,128)(2,1)} async-done(((bf16[384,512]{1,0:T(8,128)(2,1)}), bf16[384,2048]{1,0:T(8,128)(2,1)}) %all-gather.7.cloned.1.call-update) | async-done | bytes 1572880 | tf_op jit(solution)/shard_map/all_gather | solution.py:35
  31.3 1.8 fusion
  33.1 60.4 %all-gather.11.cloned.1.call-done = bf16[3,2048,256]{2,1,0:T(8,128)(2,1)} async-done(((bf16[3,256,256]{2,1,0:T(8,128)(2,1)}), bf16[3,2048,256]{2,1,0:T(8,128)(2,1)}) %all-gather.11.cloned.1.call-update) | async-done | bytes 3145744 | tf_op jit(solution)/shard_map/all_gather | solution.py:31
  93.5 2.5 fusion.13
  96.0 0.0 copy-start.7
  96.0 58.4 %all-gather.9.cloned.1.call-done = bf16[3,2048,256]{2,1,0:T(8,128)(2,1)} async-done(((bf16[3,256,256]{2,1,0:T(8,128)(2,1)}), bf16[3,2048,256]{2,1,0:T(8,128)(2,1)}) %all-gather.9.cloned.1.call-update) | async-done | bytes 3145744 | tf_op jit(solution)/shard_map/all_gather | solution.py:30
  154.4 1.9 fusion.18
  156.3 2.5 collective-permute-start
  158.8 1.3 collective-permute-start.1
  160.1 0.0 collective-permute-done
  160.1 4.6 %collective-permute-done.1 = bf16[15,256]{1,0:T(8,128)(2,1)S(1)} collective-permute-done((bf16[15,256]{1,0:T(8,128)(2,1)S(1)}, bf16[15,256]{1,0:T(8,128)(2,1)S(1)}, u32[]{:S(2)}, u32[]{:S(2)}) %collective-permute-start.1) | collective-permute-done | bytes 7712 | tf_op jit(solution)/shard_map/ppermute | solution.py:17
  164.7 1.7 fusion.140
  166.4 6.2 %all-reduce.2 = (f32[384,1]{0,1:T(1,128)S(1)}, f32[384,1]{0,1:T(1,128)S(1)}) all-reduce(f32[384,1]{0,1:T(1,128)S(1)} %broadcast_in_dim.21, f32[384,1]{0,1:T(1,128)S(1)} %broadcast_in_dim.22), channel_id=1, replica_groups=mesh['sp'=8,'tp'=4] {'tp'}, use_global_device_ids=true, to_apply=%region_2.0 | all-reduce | flops 768 | bytes 6144 | tf_op jit(solution)/shard_map/psum | solution.py:49
  172.7 45.0 %all-gather.13.cloned.1.call-done = bf16[3,256,2048]{2,1,0:T(8,128)(2,1)} async-done(((bf16[3,256,256]{2,1,0:T(8,128)(2,1)}), bf16[3,256,2048]{2,1,0:T(8,128)(2,1)}) %all-gather.13.cloned.1.call-update) | async-done | bytes 3145744 | tf_op jit(solution)/shard_map/all_gather | solution.py:33
  217.7 3.1 convolution_convert_fusion.2
  220.8 0.0 reduce-scatter.4.cloned.1.call-update
  220.8 0.0 all-gather.15.cloned.1.call-start
  220.8 26.3 %reduce-scatter.4.cloned.1.call-done = bf16[384,512]{1,0:T(8,128)(2,1)} async-done(((bf16[384,2048]{1,0:T(8,128)(2,1)}), bf16[384,512]{1,0:T(8,128)(2,1)}) %reduce-scatter.4.cloned.1.call-update) | async-done | bytes 393232 | tf_op jit(solution)/shard_map/reduce_scatter | solution.py:65
  247.2 1.8 add_convert_fusion.2
  249.0 0.0 all-gather.15.cloned.1.call-update
  249.0 0.0 reduce-scatter.6.cloned.1.call-start
  249.1 19.7 %all-gather.15.cloned.1.call-done = bf16[384,2048]{1,0:T(8,128)(2,1)} async-done(((bf16[384,512]{1,0:T(8,128)(2,1)}), bf16[384,2048]{1,0:T(8,128)(2,1)}) %all-gather.15.cloned.1.call-update) | async-done | bytes 1572880 | tf_op jit(solution)/shard_map/all_gather | solution.py:35
  268.8 1.8 fusion.3
  270.6 2.5 fusion.15
  273.1 1.9 fusion.19
  275.0 3.4 collective-permute-start.2
  278.4 1.3 collective-permute-start.3
  279.7 0.0 collective-permute-done.2
  279.7 4.2 %collective-permute-done.3 = bf16[15,256]{1,0:T(8,128)(2,1)S(1)} collective-permute-done((bf16[15,256]{1,0:T(8,128)(2,1)S(1)}, bf16[15,256]{1,0:T(8,128)(2,1)S(1)}, u32[]{:S(2)}, u32[]{:S(2)}) %collective-permute-start.3) | collective-permute-done | bytes 7712 | tf_op jit(solution)/shard_map/ppermute | solution.py:17
  284.0 1.7 fusion.139
  285.7 6.1 %all-reduce.1 = (f32[384,1]{0,1:T(1,128)S(1)}, f32[384,1]{0,1:T(1,128)S(1)}) all-reduce(f32[384,1]{0,1:T(1,128)S(1)} %broadcast_in_dim.23, f32[384,1]{0,1:T(1,128)S(1)} %broadcast_in_dim.24), channel_id=1, replica_groups=mesh['sp'=8,'tp'=4] {'tp'}, use_global_device_ids=true, to_apply=%region_8.9 | all-reduce | flops 768 | bytes 6144 | tf_op jit(solution)/shard_map/psum | solution.py:49
  291.8 3.1 convolution_convert_fusion.1
  294.8 0.0 reduce-scatter.6.cloned.1.call-update
  294.9 0.0 all-gather.17.cloned.1.call-start
  294.9 28.1 %reduce-scatter.6.cloned.1.call-done = bf16[384,512]{1,0:T(8,128)(2,1)} async-done(((bf16[384,2048]{1,0:T(8,128)(2,1)}), bf16[384,512]{1,0:T(8,128)(2,1)}) %reduce-scatter.6.cloned.1.call-update) | async-done | bytes 393232 | tf_op jit(solution)/shard_map/reduce_scatter | solution.py:65
  323.0 1.8 add_convert_fusion.1
  324.8 0.0 all-gather.17.cloned.1.call-update
  324.9 0.0 reduce-scatter.8.cloned.1.call-start
  324.9 19.7 %all-gather.17.cloned.1.call-done = bf16[384,2048]{1,0:T(8,128)(2,1)} async-done(((bf16[384,512]{1,0:T(8,128)(2,1)}), bf16[384,2048]{1,0:T(8,128)(2,1)}) %all-gather.17.cloned.1.call-update) | async-done | bytes 1572880 | tf_op jit(solution)/shard_map/all_gather | solution.py:35
  344.6 1.8 fusion.6
  346.4 2.5 fusion.17
  348.9 1.9 fusion.20
  350.8 3.4 collective-permute-start.4
  354.2 1.5 collective-permute-start.5
  355.7 4.0 collective-permute-done.5
  359.8 1.7 fusion.138
  361.5 6.1 %all-reduce = (f32[384,1]{0,1:T(1,128)S(1)}, f32[384,1]{0,1:T(1,128)S(1)}) all-reduce(f32[384,1]{0,1:T(1,128)S(1)} %broadcast_in_dim.25, f32[384,1]{0,1:T(1,128)S(1)} %broadcast_in_dim.26), channel_id=1, replica_groups=mesh['sp'=8,'tp'=4] {'tp'}, use_global_device_ids=true, to_apply=%region_14.15 | all-reduce | flops 768 | bytes 6144 | tf_op jit(solution)/shard_map/psum | solution.py:49
  367.6 3.0 convolution_convert_fusion
  370.6 0.0 reduce-scatter.8.cloned.1.call-update
  370.7 28.2 %reduce-scatter.8.cloned.1.call-done = bf16[384,512]{1,0:T(8,128)(2,1)} async-done(((bf16[384,2048]{1,0:T(8,128)(2,1)}), bf16[384,512]{1,0:T(8,128)(2,1)}) %reduce-scatter.8.cloned.1.call-update) | async-done | bytes 393232 | tf_op jit(solution)/shard_map/reduce_scatter | solution.py:65
  398.9 1.8 add_convert_fusion
  (39 shorter events, 0.4 us)
Async XLA Ops:
  6.5 24.7 %all-gather.7.cloned.1.call-start = ((), (), s32[]{:S(2)}) async-start(), calls=%async_computation.3 | async-start | bytes 1966080 | tf_op jit(solution)/shard_map/all_gather | solution.py:35
  7.3 86.3 %all-gather.11.cloned.1.call-start = ((), (), s32[]{:S(2)}) async-start(), calls=%async_computation.5 | async-start | bytes 3538944 | tf_op jit(solution)/shard_map/all_gather | solution.py:31
  8.0 146.4 %all-gather.9.cloned.1.call-start = ((), (), s32[]{:S(2)}) async-start(), calls=%async_computation.4 | async-start | bytes 3538944 | tf_op jit(solution)/shard_map/all_gather | solution.py:30
  8.7 208.9 %all-gather.13.cloned.1.call-start = ((), (), s32[]{:S(2)}) async-start(), calls=%async_computation.6 | async-start | bytes 3538944 | tf_op jit(solution)/shard_map/all_gather | solution.py:33
  9.3 237.9 %reduce-scatter.4.cloned.1.call-start = ((), (), s32[]{:S(2)}) async-start(), calls=%async_computation.7 | async-start | bytes 1966080 | tf_op jit(solution)/shard_map/reduce_scatter | solution.py:65
  93.5 60.9 %copy-start.2 = (bf16[384,2048]{1,0:T(8,128)(2,1)S(1)}, bf16[384,2048]{1,0:T(8,128)(2,1)}, u32[]{:S(2)}) copy-start(bf16[384,2048]{1,0:T(8,128)(2,1)} %all-gather.7.cloned.1.call-done) | copy-start | bytes 4718596
  96.0 64.1 %copy-start.7 = (f32[3,256]{1,0:T(4,128)S(1)}, f32[3,256]{1,0:T(4,128)}, u32[]{:S(2)}) copy-start(f32[3,256]{1,0:T(4,128)} %param.16) | copy-start | bytes 9220
  156.3 3.8 collective-permute-start
  158.8 5.9 %collective-permute-start.1 = (bf16[15,256]{1,0:T(8,128)(2,1)S(1)}, bf16[15,256]{1,0:T(8,128)(2,1)S(1)}, u32[]{:S(2)}, u32[]{:S(2)}) collective-permute-start(bf16[15,256]{1,0:T(8,128)(2,1)S(1)} %get-tuple-element.31), channel_id=1, source_target_pairs={{4,0},{8,4},{12,8},{16,12},{20,16},{24,20},{28,24},{5,1},{9,5},{13... | collective-permute-start | bytes 23048 | tf_op jit(solution)/shard_map/ppermute | solution.py:17
  166.4 80.7 %copy-start.5 = (bf16[384,512]{1,0:T(8,128)(2,1)S(1)}, bf16[384,512]{1,0:T(8,128)(2,1)}, u32[]{:S(2)}) copy-start(bf16[384,512]{1,0:T(8,128)(2,1)} %param.9) | copy-start | bytes 1179652
  217.7 31.4 %copy-start.6 = (f32[3,31,256]{2,1,0:T(8,128)S(1)}, f32[3,31,256]{2,1,0:T(8,128)}, u32[]{:S(2)}) copy-start(f32[3,31,256]{2,1,0:T(8,128)} %param.13) | copy-start | bytes 285700
  220.8 48.0 %all-gather.15.cloned.1.call-start = ((), (), s32[]{:S(2)}) async-start(), calls=%async_computation.8 | async-start | bytes 1966080 | tf_op jit(solution)/shard_map/all_gather | solution.py:35
  249.0 74.0 %reduce-scatter.6.cloned.1.call-start = ((), (), s32[]{:S(2)}) async-start(), calls=%async_computation.9 | async-start | bytes 1966080 | tf_op jit(solution)/shard_map/reduce_scatter | solution.py:65
  270.6 2.5 copy-start.3
  275.0 4.7 %collective-permute-start.2 = (bf16[15,256]{1,0:T(8,128)(2,1)S(1)}, bf16[15,256]{1,0:T(8,128)(2,1)S(1)}, u32[]{:S(2)}, u32[]{:S(2)}) collective-permute-start(bf16[15,256]{1,0:T(8,128)(2,1)S(1)} %get-tuple-element.28), channel_id=1, source_target_pairs={{0,4},{4,8},{8,12},{12,16},{16,20},{20,24},{24,28},{1,5},{5,9},{9,... | collective-permute-start | bytes 23048 | tf_op jit(solution)/shard_map/ppermute | solution.py:16
  278.4 5.5 %collective-permute-start.3 = (bf16[15,256]{1,0:T(8,128)(2,1)S(1)}, bf16[15,256]{1,0:T(8,128)(2,1)S(1)}, u32[]{:S(2)}, u32[]{:S(2)}) collective-permute-start(bf16[15,256]{1,0:T(8,128)(2,1)S(1)} %get-tuple-element.29), channel_id=1, source_target_pairs={{4,0},{8,4},{12,8},{16,12},{20,16},{24,20},{28,24},{5,1},{9,5},{13... | collective-permute-start | bytes 23048 | tf_op jit(solution)/shard_map/ppermute | solution.py:17
  285.7 37.3 %copy-start = (bf16[384,512]{1,0:T(8,128)(2,1)S(1)}, bf16[384,512]{1,0:T(8,128)(2,1)}, u32[]{:S(2)}) copy-start(bf16[384,512]{1,0:T(8,128)(2,1)} %add_convert_fusion.2) | copy-start | bytes 1179652
  294.9 49.8 %all-gather.17.cloned.1.call-start = ((), (), s32[]{:S(2)}) async-start(), calls=%async_computation.10 | async-start | bytes 1966080 | tf_op jit(solution)/shard_map/all_gather | solution.py:35
  324.9 74.0 %reduce-scatter.8.cloned.1.call-start = ((), (), s32[]{:S(2)}) async-start(), calls=%async_computation.11 | async-start | bytes 1966080 | tf_op jit(solution)/shard_map/reduce_scatter | solution.py:65
  346.4 2.5 copy-start.4
  350.8 4.9 %collective-permute-start.4 = (bf16[15,256]{1,0:T(8,128)(2,1)S(1)}, bf16[15,256]{1,0:T(8,128)(2,1)S(1)}, u32[]{:S(2)}, u32[]{:S(2)}) collective-permute-start(bf16[15,256]{1,0:T(8,128)(2,1)S(1)} %get-tuple-element.26), channel_id=1, source_target_pairs={{0,4},{4,8},{8,12},{12,16},{16,20},{20,24},{24,28},{1,5},{5,9},{9,... | collective-permute-start | bytes 23048 | tf_op jit(solution)/shard_map/ppermute | solution.py:16
  354.2 5.5 %collective-permute-start.5 = (bf16[15,256]{1,0:T(8,128)(2,1)S(1)}, bf16[15,256]{1,0:T(8,128)(2,1)S(1)}, u32[]{:S(2)}, u32[]{:S(2)}) collective-permute-start(bf16[15,256]{1,0:T(8,128)(2,1)S(1)} %get-tuple-element.27), channel_id=1, source_target_pairs={{4,0},{8,4},{12,8},{16,12},{20,16},{24,20},{28,24},{5,1},{9,5},{13... | collective-permute-start | bytes 23048 | tf_op jit(solution)/shard_map/ppermute | solution.py:17
  361.5 37.4 %copy-start.1 = (bf16[384,512]{1,0:T(8,128)(2,1)S(1)}, bf16[384,512]{1,0:T(8,128)(2,1)}, u32[]{:S(2)}) copy-start(bf16[384,512]{1,0:T(8,128)(2,1)} %add_convert_fusion.1) | copy-start | bytes 1179652
Sparse Core Ops, SparseCore 0:
  8.9 22.3 all-gather.6
  33.5 60.0 all-gather.10
  95.7 58.6 all-gather.8
  156.3 61.2 all-gather.12
  220.9 26.2 reduce-scatter.3
  249.2 19.6 all-gather.14
  295.0 27.9 reduce-scatter.5
  325.0 19.6 all-gather.16
  370.8 28.0 reduce-scatter.7
where the time goes:
time: 408 us; the launch traced here: 407 us
  waiting for transfers between devices  319 us (78%)
  matrix products  22.1 us (5%)
  blocking collectives  18.4 us (5%)
  other arithmetic  16.2 us (4%)
  starting transfers between devices  13.6 us (3%)
  between operations  13.5 us (3%)
  local copies, waits for them, and re-layouts  4.71 us (1%)
    reduce_scatter x3, waiting for transfers between devices, body(): lax.psum_scatter(partial_rows.astype(jnp.bfloat16), 'tp', scatter_dimensi...  82.6 us
    all_gather x1, waiting for transfers between devices, body(): lax.all_gather(w_gate, 'sp', axis=1, tiled=True)  60.4 us
    all_gather x1, waiting for transfers between devices, body(): lax.all_gather(w_value, 'sp', axis=1, tiled=True)  58.4 us
    all_gather x3, waiting for transfers between devices, body(): whole_rows = lax.all_gather(stream, 'tp', axis=1, tiled=True)  56.8 us
    all_gather x1, waiting for transfers between devices, body(): whole_out = lax.all_gather(w_out, 'sp', axis=2, tiled=True)  45 us
    psum x3, blocking collectives, body(): lax.psum((jnp.sum(convolved, axis=-1, keepdims=True), jnp.sum(convolved *...  18.4 us
    ppermute x3, waiting for transfers between devices, with_halo(): after = lax.ppermute(first, axis, down)  12.8 us
    ppermute x3, starting transfers between devices, with_halo(): before = lax.ppermute(last, axis, up)  9.21 us
  transfers between devices with their start and end apart: 15, of which 12 were waited for; matrix products, arithmetic and copies ran while one was open for 3% of the time, Pallas kernels for 0%

commit v1 on v0

--- a/solution.py
+++ b/solution.py
@@ -30,7 +30,12 @@
         lax.all_gather(w_value, "sp", axis=1, tiled=True),
         lax.all_gather(w_gate, "sp", axis=1, tiled=True),
     )
-    whole_out = lax.all_gather(w_out, "sp", axis=2, tiled=True)
+    ring = [w_out]
+    for hop in range(7):
+        ring.append(lax.ppermute(ring[-1], "sp", [(dev, (dev + 1) % 8) for dev in range(8)]))
+    whole_out = jnp.roll(
+        jnp.concatenate(ring[::-1], axis=2), (lax.axis_index("sp") + 1) * ring[0].shape[2], axis=2
+    )
     for layer_index in range(layer_count):
         whole_rows = lax.all_gather(stream, "tp", axis=1, tiled=True)
         rows_f32 = whole_rows.astype(jnp.float32)

time: 408 us -> 392 us (0.961)
  waiting for transfers between devices: 319 us -> 274 us
  local copies, waits for them, and re-layouts: 4.71 us -> 25.5 us
  starting transfers between devices: 13.6 us -> 21 us
    ppermute x0 -> x7, waiting for transfers between devices: none -> 99.7 us  [body(): lax.ppermute(ring[-1], 'sp', [(dev, (dev + 1) % 8) for dev in range(8)])]
    all_gather x1, waiting for transfers between devices: 60.4 us -> 0.01 us  [body(): lax.all_gather(w_gate, 'sp', axis=1, tiled=True)]
    all_gather x1 -> x0, waiting for transfers between devices: 45 us -> none  [body(): whole_out = lax.all_gather(w_out, 'sp', axis=2, tiled=True)]
    all_gather x1, waiting for transfers between devices: 58.4 us -> 39.5 us  [body(): lax.all_gather(w_value, 'sp', axis=1, tiled=True)]
    all_gather x3, waiting for transfers between devices: 56.8 us -> 39.3 us  [body(): whole_rows = lax.all_gather(stream, 'tp', axis=1, tiled=True)]
    unnamed x16 -> x131, local copies, waits for them, and re-layouts: 0.03 us -> 15.6 us
    ppermute x3, waiting for transfers between devices: 12.8 us -> 0.01 us  [with_halo(): after = lax.ppermute(first, axis, down)]
    reduce_scatter x3, waiting for transfers between devices: 82.6 us -> 89.8 us  [body(): lax.psum_scatter(partial_rows.astype(jnp.bfloat16), 'tp', scatter_dimensi...]
  transfers between devices with their start and end apart: 15 -> 21, of which waited for: 12 -> 16; matrix products, arithmetic and copies ran while one was open for 3% -> 8% of each run, Pallas kernels for 0% -> 0%
where the time goes in v1:
time: 392 us; the launch traced here: 390 us
  waiting for transfers between devices  274 us (70%)
  local copies, waits for them, and re-layouts  25.5 us (7%)
  matrix products  21.7 us (6%)
  starting transfers between devices  21 us (5%)
  blocking collectives  17.3 us (4%)
  other arithmetic  16.9 us (4%)
  between operations  14.5 us (4%)
    ppermute x7, waiting for transfers between devices, body(): lax.ppermute(ring[-1], 'sp', [(dev, (dev + 1) % 8) for dev in range(8)])  99.7 us
    reduce_scatter x3, waiting for transfers between devices, body(): lax.psum_scatter(partial_rows.astype(jnp.bfloat16), 'tp', scatter_dimensi...  89.8 us
    all_gather x1, waiting for transfers between devices, body(): lax.all_gather(w_value, 'sp', axis=1, tiled=True)  39.5 us
    all_gather x3, waiting for transfers between devices, body(): whole_rows = lax.all_gather(stream, 'tp', axis=1, tiled=True)  39.3 us
    psum x3, blocking collectives, body(): lax.psum((jnp.sum(convolved, axis=-1, keepdims=True), jnp.sum(convolved *...  17.3 us
    unnamed x131, local copies, waits for them, and re-layouts  15.6 us
    ppermute x3, starting transfers between devices, with_halo(): before = lax.ppermute(last, axis, up)  13.6 us
    dot_general x3, matrix products, body(): jnp.dot(activated, whole_out[layer_index], preferred_element_type=jnp.flo...  9.31 us
  transfers between devices with their start and end apart: 21, of which 16 were waited for; matrix products, arithmetic and copies ran while one was open for 8% of the time, Pallas kernels for 0%

profile of v1, /device:TPU:0, one launch (start us, length us, event | category | flops | bytes accessed | tf_op | source)
XLA Modules:
  0.0 390.5 jit_solution(5175920986549088997)
XLA Ops:
  8.8 3.0 collective-permute-start.2
  11.8 12.4 %collective-permute-done.2 = bf16[3,256,256]{2,1,0:T(8,128)(2,1)S(1)} collective-permute-done((bf16[3,256,256]{2,1,0:T(8,128)(2,1)}, bf16[3,256,256]{2,1,0:T(8,128)(2,1)S(1)}, u32[]{:S(2)}, u32[]{:S(2)}) %collective-permute-start.2) | collective-permute-done | bytes 393248 | tf_op jit(solution)/shard_map/ppermute | solution.py:35
  24.2 13.0 %collective-permute-done.3 = bf16[3,256,256]{2,1,0:T(8,128)(2,1)S(1)} collective-permute-done((bf16[3,256,256]{2,1,0:T(8,128)(2,1)S(1)}, bf16[3,256,256]{2,1,0:T(8,128)(2,1)S(1)}, u32[]{:S(2)}, u32[]{:S(2)}) %collective-permute-start.3) | collective-permute-done | bytes 393248 | tf_op jit(solution)/shard_map/ppermute | solution.py:35
  37.2 1.3 fusion.158
  38.5 15.3 %collective-permute-done.4 = bf16[3,256,256]{2,1,0:T(8,128)(2,1)S(1)} collective-permute-done((bf16[3,256,256]{2,1,0:T(8,128)(2,1)S(1)}, bf16[3,256,256]{2,1,0:T(8,128)(2,1)S(1)}, u32[]{:S(2)}, u32[]{:S(2)}) %collective-permute-start.4) | collective-permute-done | bytes 393248 | tf_op jit(solution)/shard_map/ppermute | solution.py:35
  53.9 1.4 fusion.157
  55.2 1.7 fusion.154
  56.9 13.5 %collective-permute-done.5 = bf16[3,256,256]{2,1,0:T(8,128)(2,1)S(1)} collective-permute-done((bf16[3,256,256]{2,1,0:T(8,128)(2,1)S(1)}, bf16[3,256,256]{2,1,0:T(8,128)(2,1)S(1)}, u32[]{:S(2)}, u32[]{:S(2)}) %collective-permute-start.5) | collective-permute-done | bytes 393248 | tf_op jit(solution)/shard_map/ppermute | solution.py:35
  70.4 1.3 fusion.156
  71.7 1.7 fusion.153
  73.4 15.0 %collective-permute-done.6 = bf16[3,256,256]{2,1,0:T(8,128)(2,1)S(1)} collective-permute-done((bf16[3,256,256]{2,1,0:T(8,128)(2,1)S(1)}, bf16[3,256,256]{2,1,0:T(8,128)(2,1)S(1)}, u32[]{:S(2)}, u32[]{:S(2)}) %collective-permute-start.6) | collective-permute-done | bytes 393248 | tf_op jit(solution)/shard_map/ppermute | solution.py:35
  88.5 1.5 fusion.155
  90.0 19.8 %collective-permute-done.7 = bf16[3,256,256]{2,1,0:T(8,128)(2,1)S(1)} collective-permute-done((bf16[3,256,256]{2,1,0:T(8,128)(2,1)S(1)}, bf16[3,256,256]{2,1,0:T(8,128)(2,1)S(1)}, u32[]{:S(2)}, u32[]{:S(2)}) %collective-permute-start.7) | collective-permute-done | bytes 393248 | tf_op jit(solution)/shard_map/ppermute | solution.py:35
  109.8 1.9 fusion
  112.3 10.7 %collective-permute-done.8 = bf16[3,256,256]{2,1,0:T(8,128)(2,1)S(1)} collective-permute-done((bf16[3,256,256]{2,1,0:T(8,128)(2,1)S(1)}, bf16[3,256,256]{2,1,0:T(8,128)(2,1)S(1)}, u32[]{:S(2)}, u32[]{:S(2)}) %collective-permute-start.8) | collective-permute-done | bytes 393248 | tf_op jit(solution)/shard_map/ppermute | solution.py:35
  123.0 0.9 constant_dynamic-update-slice_fusion.15
  123.9 0.8 constant_dynamic-update-slice_fusion.14
  124.7 0.8 constant_dynamic-update-slice_fusion.13
  126.3 0.8 constant_dynamic-update-slice_fusion.11
  127.2 0.8 constant_dynamic-update-slice_fusion.10
  128.0 0.9 constant_dynamic-update-slice_fusion.9
  128.8 0.8 constant_dynamic-update-slice_fusion.8
  129.7 1.8 constant_dynamic-update-slice_fusion.7
  131.5 1.8 constant_dynamic-update-slice_fusion.6
  133.3 1.8 constant_dynamic-update-slice_fusion.5
  135.1 0.8 constant_dynamic-update-slice_fusion.4
  135.9 0.8 constant_dynamic-update-slice_fusion.3
  136.7 0.8 constant_dynamic-update-slice_fusion.2
  137.6 0.8 constant_dynamic-update-slice_fusion.1
  138.4 1.9 fusion.13
  140.7 39.5 %all-gather.8.cloned.1.call-done = bf16[3,2048,256]{2,1,0:T(8,128)(2,1)} async-done(((bf16[3,256,256]{2,1,0:T(8,128)(2,1)}), bf16[3,2048,256]{2,1,0:T(8,128)(2,1)}) %all-gather.8.cloned.1.call-update) | async-done | bytes 3145744 | tf_op jit(solution)/shard_map/all_gather | solution.py:30
  180.2 1.8 fusion.18
  182.0 1.3 collective-permute-start.1
  183.3 4.5 %collective-permute-start = (bf16[15,256]{1,0:T(8,128)(2,1)S(1)}, bf16[15,256]{1,0:T(8,128)(2,1)S(1)}, u32[]{:S(2)}, u32[]{:S(2)}) collective-permute-start(bf16[15,256]{1,0:T(8,128)(2,1)S(1)} %get-tuple-element.30), channel_id=1, source_target_pairs={{0,4},{4,8},{8,12},{12,16},{16,20},{20,24},{24,28},{1,5},{5,9},{9,... | collective-permute-start | bytes 23048 | tf_op jit(solution)/shard_map/ppermute | solution.py:16
  187.9 0.8 constant_dynamic-update-slice_fusion
  189.6 1.7 fusion.143
  191.3 5.8 %all-reduce.2 = (f32[384,1]{0,1:T(1,128)S(1)}, f32[384,1]{0,1:T(1,128)S(1)}) all-reduce(f32[384,1]{0,1:T(1,128)S(1)} %broadcast_in_dim.21, f32[384,1]{0,1:T(1,128)S(1)} %broadcast_in_dim.22), channel_id=1, replica_groups=mesh['sp'=8,'tp'=4] {'tp'}, use_global_device_ids=true, to_apply=%region_2.3 | all-reduce | flops 768 | bytes 6144 | tf_op jit(solution)/shard_map/psum | solution.py:54
  197.2 3.1 convolution_convert_fusion.2
  200.3 29.6 %reduce-scatter.4.cloned.1.call-done = bf16[384,512]{1,0:T(8,128)(2,1)} async-done(((bf16[384,2048]{1,0:T(8,128)(2,1)}), bf16[384,512]{1,0:T(8,128)(2,1)}) %reduce-scatter.4.cloned.1.call-update) | async-done | bytes 393232 | tf_op jit(solution)/shard_map/reduce_scatter | solution.py:70
  230.0 1.8 add_convert_fusion.2
  231.9 19.7 %all-gather.12.cloned.1.call-done = bf16[384,2048]{1,0:T(8,128)(2,1)} async-done(((bf16[384,512]{1,0:T(8,128)(2,1)}), bf16[384,2048]{1,0:T(8,128)(2,1)}) %all-gather.12.cloned.1.call-update) | async-done | bytes 1572880 | tf_op jit(solution)/shard_map/all_gather | solution.py:40
  251.6 1.8 fusion.3
  253.4 2.5 fusion.15
  255.9 1.9 fusion.19
  257.8 1.3 collective-permute-start.10
  259.1 4.5 %collective-permute-start.9 = (bf16[15,256]{1,0:T(8,128)(2,1)S(1)}, bf16[15,256]{1,0:T(8,128)(2,1)S(1)}, u32[]{:S(2)}, u32[]{:S(2)}) collective-permute-start(bf16[15,256]{1,0:T(8,128)(2,1)S(1)} %get-tuple-element.28), channel_id=1, source_target_pairs={{0,4},{4,8},{8,12},{12,16},{16,20},{20,24},{24,28},{1,5},{5,9},{9,... | collective-permute-start | bytes 23048 | tf_op jit(solution)/shard_map/ppermute | solution.py:16
  263.7 1.3 collective-permute-done.9
  265.2 1.7 fusion.142
  266.9 5.8 %all-reduce.1 = (f32[384,1]{0,1:T(1,128)S(1)}, f32[384,1]{0,1:T(1,128)S(1)}) all-reduce(f32[384,1]{0,1:T(1,128)S(1)} %broadcast_in_dim.23, f32[384,1]{0,1:T(1,128)S(1)} %broadcast_in_dim.24), channel_id=1, replica_groups=mesh['sp'=8,'tp'=4] {'tp'}, use_global_device_ids=true, to_apply=%region_8.9 | all-reduce | flops 768 | bytes 6144 | tf_op jit(solution)/shard_map/psum | solution.py:54
  272.7 3.1 convolution_convert_fusion.1
  275.8 30.0 %reduce-scatter.6.cloned.1.call-done = bf16[384,512]{1,0:T(8,128)(2,1)} async-done(((bf16[384,2048]{1,0:T(8,128)(2,1)}), bf16[384,512]{1,0:T(8,128)(2,1)}) %reduce-scatter.6.cloned.1.call-update) | async-done | bytes 393232 | tf_op jit(solution)/shard_map/reduce_scatter | solution.py:70
  305.9 1.8 add_convert_fusion.1
  308.0 19.6 %all-gather.14.cloned.1.call-done = bf16[384,2048]{1,0:T(8,128)(2,1)} async-done(((bf16[384,512]{1,0:T(8,128)(2,1)}), bf16[384,2048]{1,0:T(8,128)(2,1)}) %all-gather.14.cloned.1.call-update) | async-done | bytes 1572880 | tf_op jit(solution)/shard_map/all_gather | solution.py:40
  327.5 1.8 fusion.6
  329.3 2.5 fusion.17
  331.8 1.9 fusion.20
  333.7 1.3 collective-permute-start.12
  335.0 4.5 %collective-permute-start.11 = (bf16[15,256]{1,0:T(8,128)(2,1)S(1)}, bf16[15,256]{1,0:T(8,128)(2,1)S(1)}, u32[]{:S(2)}, u32[]{:S(2)}) collective-permute-start(bf16[15,256]{1,0:T(8,128)(2,1)S(1)} %get-tuple-element.26), channel_id=1, source_target_pairs={{0,4},{4,8},{8,12},{12,16},{16,20},{20,24},{24,28},{1,5},{5,9},{9,... | collective-permute-start | bytes 23048 | tf_op jit(solution)/shard_map/ppermute | solution.py:16
  339.6 1.3 collective-permute-done.11
  341.0 1.7 fusion.141
  342.7 5.8 %all-reduce = (f32[384,1]{0,1:T(1,128)S(1)}, f32[384,1]{0,1:T(1,128)S(1)}) all-reduce(f32[384,1]{0,1:T(1,128)S(1)} %broadcast_in_dim.25, f32[384,1]{0,1:T(1,128)S(1)} %broadcast_in_dim.26), channel_id=1, replica_groups=mesh['sp'=8,'tp'=4] {'tp'}, use_global_device_ids=true, to_apply=%region_14.15 | all-reduce | flops 768 | bytes 6144 | tf_op jit(solution)/shard_map/psum | solution.py:54
  348.5 3.2 convolution_convert_fusion
  351.7 30.1 %reduce-scatter.8.cloned.1.call-done = bf16[384,512]{1,0:T(8,128)(2,1)} async-done(((bf16[384,2048]{1,0:T(8,128)(2,1)}), bf16[384,512]{1,0:T(8,128)(2,1)}) %reduce-scatter.8.cloned.1.call-update) | async-done | bytes 393232 | tf_op jit(solution)/shard_map/reduce_scatter | solution.py:70
  381.8 1.8 add_convert_fusion
  (166 shorter events, 5.2 us)
Async XLA Ops:
  6.5 103.2 %all-gather.6.cloned.1.call-start = ((), (), s32[]{:S(2)}) async-start(), calls=%async_computation.3 | async-start | bytes 1966080 | tf_op jit(solution)/shard_map/all_gather | solution.py:40
  7.3 131.2 %all-gather.10.cloned.1.call-start = ((), (), s32[]{:S(2)}) async-start(), calls=%async_computation.5 | async-start | bytes 3538944 | tf_op jit(solution)/shard_map/all_gather | solution.py:31
  8.0 172.1 %all-gather.8.cloned.1.call-start = ((), (), s32[]{:S(2)}) async-start(), calls=%async_computation.4 | async-start | bytes 3538944 | tf_op jit(solution)/shard_map/all_gather | solution.py:30
  8.7 221.2 %reduce-scatter.4.cloned.1.call-start = ((), (), s32[]{:S(2)}) async-start(), calls=%async_computation.6 | async-start | bytes 1966080 | tf_op jit(solution)/shard_map/reduce_scatter | solution.py:70
  8.8 15.4 %collective-permute-start.2 = (bf16[3,256,256]{2,1,0:T(8,128)(2,1)}, bf16[3,256,256]{2,1,0:T(8,128)(2,1)S(1)}, u32[]{:S(2)}, u32[]{:S(2)}) collective-permute-start(bf16[3,256,256]{2,1,0:T(8,128)(2,1)} %param.17), channel_id=1, source_target_pairs={{0,4},{4,8},{8,12},{12,16},{16,20},{20,24},{24,28},{28,0},{1,5},{5... | collective-permute-start | bytes 1179656 | tf_op jit(solution)/shard_map/ppermute | solution.py:35
  24.2 13.0 %collective-permute-start.3 = (bf16[3,256,256]{2,1,0:T(8,128)(2,1)S(1)}, bf16[3,256,256]{2,1,0:T(8,128)(2,1)S(1)}, u32[]{:S(2)}, u32[]{:S(2)}) collective-permute-start(bf16[3,256,256]{2,1,0:T(8,128)(2,1)S(1)} %collective-permute-done.2), channel_id=1, source_target_pairs={{0,4},{4,8},{8,12},{12,16},{16,20},{20,24},{24,28},{28,0},{1,5},{5... | collective-permute-start | bytes 1179656 | tf_op jit(solution)/shard_map/ppermute | solution.py:35
  37.2 16.7 %collective-permute-start.4 = (bf16[3,256,256]{2,1,0:T(8,128)(2,1)S(1)}, bf16[3,256,256]{2,1,0:T(8,128)(2,1)S(1)}, u32[]{:S(2)}, u32[]{:S(2)}) collective-permute-start(bf16[3,256,256]{2,1,0:T(8,128)(2,1)S(1)} %collective-permute-done.3), channel_id=1, source_target_pairs={{0,4},{4,8},{8,12},{12,16},{16,20},{20,24},{24,28},{28,0},{1,5},{5... | collective-permute-start | bytes 1179656 | tf_op jit(solution)/shard_map/ppermute | solution.py:35
  53.9 16.5 %collective-permute-start.5 = (bf16[3,256,256]{2,1,0:T(8,128)(2,1)S(1)}, bf16[3,256,256]{2,1,0:T(8,128)(2,1)S(1)}, u32[]{:S(2)}, u32[]{:S(2)}) collective-permute-start(bf16[3,256,256]{2,1,0:T(8,128)(2,1)S(1)} %collective-permute-done.4), channel_id=1, source_target_pairs={{0,4},{4,8},{8,12},{12,16},{16,20},{20,24},{24,28},{28,0},{1,5},{5... | collective-permute-start | bytes 1179656 | tf_op jit(solution)/shard_map/ppermute | solution.py:35
  70.4 18.1 %collective-permute-start.6 = (bf16[3,256,256]{2,1,0:T(8,128)(2,1)S(1)}, bf16[3,256,256]{2,1,0:T(8,128)(2,1)S(1)}, u32[]{:S(2)}, u32[]{:S(2)}) collective-permute-start(bf16[3,256,256]{2,1,0:T(8,128)(2,1)S(1)} %collective-permute-done.5), channel_id=1, source_target_pairs={{0,4},{4,8},{8,12},{12,16},{16,20},{20,24},{24,28},{28,0},{1,5},{5... | collective-permute-start | bytes 1179656 | tf_op jit(solution)/shard_map/ppermute | solution.py:35
  88.5 39.5 %copy-start.6 = (bf16[3,256,256]{2,1,0:T(8,128)(2,1)}, bf16[3,256,256]{2,1,0:T(8,128)(2,1)S(1)}, u32[]{:S(2)}) copy-start(bf16[3,256,256]{2,1,0:T(8,128)(2,1)S(1)} %collective-permute-done.6) | copy-start | bytes 1179652
  88.5 21.3 %collective-permute-start.7 = (bf16[3,256,256]{2,1,0:T(8,128)(2,1)S(1)}, bf16[3,256,256]{2,1,0:T(8,128)(2,1)S(1)}, u32[]{:S(2)}, u32[]{:S(2)}) collective-permute-start(bf16[3,256,256]{2,1,0:T(8,128)(2,1)S(1)} %collective-permute-done.6), channel_id=1, source_target_pairs={{0,4},{4,8},{8,12},{12,16},{16,20},{20,24},{24,28},{28,0},{1,5},{5... | collective-permute-start | bytes 1179656 | tf_op jit(solution)/shard_map/ppermute | solution.py:35
  109.8 18.2 %copy-start.7 = (bf16[3,256,256]{2,1,0:T(8,128)(2,1)}, bf16[3,256,256]{2,1,0:T(8,128)(2,1)S(1)}, u32[]{:S(2)}) copy-start(bf16[3,256,256]{2,1,0:T(8,128)(2,1)S(1)} %collective-permute-done.7) | copy-start | bytes 1179652
  109.8 13.3 %collective-permute-start.8 = (bf16[3,256,256]{2,1,0:T(8,128)(2,1)S(1)}, bf16[3,256,256]{2,1,0:T(8,128)(2,1)S(1)}, u32[]{:S(2)}, u32[]{:S(2)}) collective-permute-start(bf16[3,256,256]{2,1,0:T(8,128)(2,1)S(1)} %collective-permute-done.7), channel_id=1, source_target_pairs={{0,4},{4,8},{8,12},{12,16},{16,20},{20,24},{24,28},{28,0},{1,5},{5... | collective-permute-start | bytes 1179656 | tf_op jit(solution)/shard_map/ppermute | solution.py:35
  111.7 17.1 %copy-start.5 = (bf16[3,256,256]{2,1,0:T(8,128)(2,1)S(1)}, bf16[3,256,256]{2,1,0:T(8,128)(2,1)}, u32[]{:S(2)}) copy-start(bf16[3,256,256]{2,1,0:T(8,128)(2,1)} %param.17) | copy-start | bytes 1179652
  128.8 9.6 %copy-start.2 = (bf16[384,2048]{1,0:T(8,128)(2,1)S(1)}, bf16[384,2048]{1,0:T(8,128)(2,1)}, u32[]{:S(2)}) copy-start(bf16[384,2048]{1,0:T(8,128)(2,1)} %all-gather.6.cloned.1.call-done) | copy-start | bytes 4718596
  138.4 41.7 %copy-start.11 = (f32[1,2048]{1,0:T(1,128)S(1)}, f32[1,2048]{1,0:T(1,128)}, u32[]{:S(2)}) copy-start(f32[1,2048]{1,0:T(1,128)} %get-tuple-element.126) | copy-start | bytes 24580
  138.4 41.7 %copy-start.51 = (f32[384]{0:T(512)S(1)}, f32[384]{0:T(512)}, u32[]{:S(2)}) copy-start(f32[384]{0:T(512)} %add_rsqrt_fusion.2) | copy-start | bytes 4612
  140.3 48.9 %copy-start.17 = (f32[1,1,256]{2,1,0:T(1,128)S(1)}, f32[1,1,256]{2,1,0:T(1,128)}, u32[]{:S(2)}) copy-start(f32[1,1,256]{2,1,0:T(1,128)} %get-tuple-element.108) | copy-start | bytes 3076
  140.3 48.9 %copy-start.18 = (f32[1,1,256]{2,1,0:T(1,128)S(1)}, f32[1,1,256]{2,1,0:T(1,128)}, u32[]{:S(2)}) copy-start(f32[1,1,256]{2,1,0:T(1,128)} %get-tuple-element.109) | copy-start | bytes 3076
  140.4 48.9 %copy-start.19 = (f32[1,1,256]{2,1,0:T(1,128)S(1)}, f32[1,1,256]{2,1,0:T(1,128)}, u32[]{:S(2)}) copy-start(f32[1,1,256]{2,1,0:T(1,128)} %get-tuple-element.110) | copy-start | bytes 3076
  140.4 48.9 %copy-start.20 = (f32[1,1,256]{2,1,0:T(1,128)S(1)}, f32[1,1,256]{2,1,0:T(1,128)}, u32[]{:S(2)}) copy-start(f32[1,1,256]{2,1,0:T(1,128)} %get-tuple-element.111) | copy-start | bytes 3076
  140.4 48.9 %copy-start.21 = (f32[1,1,256]{2,1,0:T(1,128)S(1)}, f32[1,1,256]{2,1,0:T(1,128)}, u32[]{:S(2)}) copy-start(f32[1,1,256]{2,1,0:T(1,128)} %get-tuple-element.112) | copy-start | bytes 3076
  140.4 48.9 %copy-start.22 = (f32[1,1,256]{2,1,0:T(1,128)S(1)}, f32[1,1,256]{2,1,0:T(1,128)}, u32[]{:S(2)}) copy-start(f32[1,1,256]{2,1,0:T(1,128)} %get-tuple-element.113) | copy-start | bytes 3076
  140.4 48.9 %copy-start.23 = (f32[1,1,256]{2,1,0:T(1,128)S(1)}, f32[1,1,256]{2,1,0:T(1,128)}, u32[]{:S(2)}) copy-start(f32[1,1,256]{2,1,0:T(1,128)} %get-tuple-element.114) | copy-start | bytes 3076
  140.4 48.9 %copy-start.24 = (f32[1,1,256]{2,1,0:T(1,128)S(1)}, f32[1,1,256]{2,1,0:T(1,128)}, u32[]{:S(2)}) copy-start(f32[1,1,256]{2,1,0:T(1,128)} %get-tuple-element.115) | copy-start | bytes 3076
  140.4 48.9 %copy-start.25 = (f32[1,1,256]{2,1,0:T(1,128)S(1)}, f32[1,1,256]{2,1,0:T(1,128)}, u32[]{:S(2)}) copy-start(f32[1,1,256]{2,1,0:T(1,128)} %get-tuple-element.116) | copy-start | bytes 3076
  140.4 48.9 %copy-start.26 = (f32[1,1,256]{2,1,0:T(1,128)S(1)}, f32[1,1,256]{2,1,0:T(1,128)}, u32[]{:S(2)}) copy-start(f32[1,1,256]{2,1,0:T(1,128)} %get-tuple-element.117) | copy-start | bytes 3076
  140.4 48.9 %copy-start.27 = (f32[1,1,256]{2,1,0:T(1,128)S(1)}, f32[1,1,256]{2,1,0:T(1,128)}, u32[]{:S(2)}) copy-start(f32[1,1,256]{2,1,0:T(1,128)} %get-tuple-element.118) | copy-start | bytes 3076
  140.4 48.9 %copy-start.28 = (f32[1,1,256]{2,1,0:T(1,128)S(1)}, f32[1,1,256]{2,1,0:T(1,128)}, u32[]{:S(2)}) copy-start(f32[1,1,256]{2,1,0:T(1,128)} %get-tuple-element.119) | copy-start | bytes 3076
  140.5 48.9 %copy-start.29 = (f32[1,1,256]{2,1,0:T(1,128)S(1)}, f32[1,1,256]{2,1,0:T(1,128)}, u32[]{:S(2)}) copy-start(f32[1,1,256]{2,1,0:T(1,128)} %get-tuple-element.120) | copy-start | bytes 3076
  140.5 48.9 %copy-start.30 = (f32[1,1,256]{2,1,0:T(1,128)S(1)}, f32[1,1,256]{2,1,0:T(1,128)}, u32[]{:S(2)}) copy-start(f32[1,1,256]{2,1,0:T(1,128)} %get-tuple-element.121) | copy-start | bytes 3076
  140.5 48.9 %copy-start.31 = (f32[1,1,256]{2,1,0:T(1,128)S(1)}, f32[1,1,256]{2,1,0:T(1,128)}, u32[]{:S(2)}) copy-start(f32[1,1,256]{2,1,0:T(1,128)} %get-tuple-element.122) | copy-start | bytes 3076
  140.5 48.9 %copy-start.32 = (f32[1,1,256]{2,1,0:T(1,128)S(1)}, f32[1,1,256]{2,1,0:T(1,128)}, u32[]{:S(2)}) copy-start(f32[1,1,256]{2,1,0:T(1,128)} %get-tuple-element.123) | copy-start | bytes 3076
  140.5 48.9 %copy-start.33 = (f32[1,1,256]{2,1,0:T(1,128)S(1)}, f32[1,1,256]{2,1,0:T(1,128)}, u32[]{:S(2)}) copy-start(f32[1,1,256]{2,1,0:T(1,128)} %get-tuple-element.124) | copy-start | bytes 3076
  140.5 48.9 %copy-start.34 = (f32[1,1,256]{2,1,0:T(1,128)S(1)}, f32[1,1,256]{2,1,0:T(1,128)}, u32[]{:S(2)}) copy-start(f32[1,1,256]{2,1,0:T(1,128)} %get-tuple-element.94) | copy-start | bytes 3076
  140.5 48.9 %copy-start.35 = (f32[1,1,256]{2,1,0:T(1,128)S(1)}, f32[1,1,256]{2,1,0:T(1,128)}, u32[]{:S(2)}) copy-start(f32[1,1,256]{2,1,0:T(1,128)} %get-tuple-element.95) | copy-start | bytes 3076
  140.5 48.9 %copy-start.36 = (f32[1,1,256]{2,1,0:T(1,128)S(1)}, f32[1,1,256]{2,1,0:T(1,128)}, u32[]{:S(2)}) copy-start(f32[1,1,256]{2,1,0:T(1,128)} %get-tuple-element.96) | copy-start | bytes 3076
  140.5 48.9 %copy-start.37 = (f32[1,1,256]{2,1,0:T(1,128)S(1)}, f32[1,1,256]{2,1,0:T(1,128)}, u32[]{:S(2)}) copy-start(f32[1,1,256]{2,1,0:T(1,128)} %get-tuple-element.97) | copy-start | bytes 3076
  140.5 48.9 %copy-start.38 = (f32[1,1,256]{2,1,0:T(1,128)S(1)}, f32[1,1,256]{2,1,0:T(1,128)}, u32[]{:S(2)}) copy-start(f32[1,1,256]{2,1,0:T(1,128)} %get-tuple-element.98) | copy-start | bytes 3076
  140.6 48.9 %copy-start.39 = (f32[1,1,256]{2,1,0:T(1,128)S(1)}, f32[1,1,256]{2,1,0:T(1,128)}, u32[]{:S(2)}) copy-start(f32[1,1,256]{2,1,0:T(1,128)} %get-tuple-element.99) | copy-start | bytes 3076
  140.6 48.9 %copy-start.40 = (f32[1,1,256]{2,1,0:T(1,128)S(1)}, f32[1,1,256]{2,1,0:T(1,128)}, u32[]{:S(2)}) copy-start(f32[1,1,256]{2,1,0:T(1,128)} %get-tuple-element.100) | copy-start | bytes 3076
  140.6 48.9 %copy-start.41 = (f32[1,1,256]{2,1,0:T(1,128)S(1)}, f32[1,1,256]{2,1,0:T(1,128)}, u32[]{:S(2)}) copy-start(f32[1,1,256]{2,1,0:T(1,128)} %get-tuple-element.101) | copy-start | bytes 3076
  140.6 48.9 %copy-start.42 = (f32[1,1,256]{2,1,0:T(1,128)S(1)}, f32[1,1,256]{2,1,0:T(1,128)}, u32[]{:S(2)}) copy-start(f32[1,1,256]{2,1,0:T(1,128)} %get-tuple-element.102) | copy-start | bytes 3076
  140.6 48.9 %copy-start.43 = (f32[1,1,256]{2,1,0:T(1,128)S(1)}, f32[1,1,256]{2,1,0:T(1,128)}, u32[]{:S(2)}) copy-start(f32[1,1,256]{2,1,0:T(1,128)} %get-tuple-element.103) | copy-start | bytes 3076
  140.6 48.9 %copy-start.44 = (f32[1,1,256]{2,1,0:T(1,128)S(1)}, f32[1,1,256]{2,1,0:T(1,128)}, u32[]{:S(2)}) copy-start(f32[1,1,256]{2,1,0:T(1,128)} %get-tuple-element.104) | copy-start | bytes 3076
  140.6 48.9 %copy-start.45 = (f32[1,1,256]{2,1,0:T(1,128)S(1)}, f32[1,1,256]{2,1,0:T(1,128)}, u32[]{:S(2)}) copy-start(f32[1,1,256]{2,1,0:T(1,128)} %get-tuple-element.105) | copy-start | bytes 3076
  140.6 48.9 %copy-start.46 = (f32[1,1,256]{2,1,0:T(1,128)S(1)}, f32[1,1,256]{2,1,0:T(1,128)}, u32[]{:S(2)}) copy-start(f32[1,1,256]{2,1,0:T(1,128)} %get-tuple-element.106) | copy-start | bytes 3076
  140.6 48.9 %copy-start.47 = (f32[1,1,256]{2,1,0:T(1,128)S(1)}, f32[1,1,256]{2,1,0:T(1,128)}, u32[]{:S(2)}) copy-start(f32[1,1,256]{2,1,0:T(1,128)} %get-tuple-element.107) | copy-start | bytes 3076
  140.6 48.9 %copy-start.50 = (f32[1,256]{1,0:T(1,128)S(1)}, f32[1,256]{1,0:T(1,128)}, u32[]{:S(2)}) copy-start(f32[1,256]{1,0:T(1,128)} %get-tuple-element.135) | copy-start | bytes 3076
  182.0 6.7 %collective-permute-start.1 = (bf16[15,256]{1,0:T(8,128)(2,1)S(1)}, bf16[15,256]{1,0:T(8,128)(2,1)S(1)}, u32[]{:S(2)}, u32[]{:S(2)}) collective-permute-start(bf16[15,256]{1,0:T(8,128)(2,1)S(1)} %get-tuple-element.31), channel_id=1, source_target_pairs={{4,0},{8,4},{12,8},{16,12},{20,16},{24,20},{28,24},{5,1},{9,5},{13... | collective-permute-start | bytes 23048 | tf_op jit(solution)/shard_map/ppermute | solution.py:17
  183.3 5.9 %collective-permute-start = (bf16[15,256]{1,0:T(8,128)(2,1)S(1)}, bf16[15,256]{1,0:T(8,128)(2,1)S(1)}, u32[]{:S(2)}, u32[]{:S(2)}) collective-permute-start(bf16[15,256]{1,0:T(8,128)(2,1)S(1)} %get-tuple-element.30), channel_id=1, source_target_pairs={{0,4},{4,8},{8,12},{12,16},{16,20},{20,24},{24,28},{1,5},{5,9},{9,... | collective-permute-start | bytes 23048 | tf_op jit(solution)/shard_map/ppermute | solution.py:16
  191.3 38.7 %copy-start.9 = (bf16[384,512]{1,0:T(8,128)(2,1)S(1)}, bf16[384,512]{1,0:T(8,128)(2,1)}, u32[]{:S(2)}) copy-start(bf16[384,512]{1,0:T(8,128)(2,1)} %param.9) | copy-start | bytes 1179652
  197.2 34.7 %copy-start.10 = (f32[3,31,256]{2,1,0:T(8,128)S(1)}, f32[3,31,256]{2,1,0:T(8,128)}, u32[]{:S(2)}) copy-start(f32[3,31,256]{2,1,0:T(8,128)} %param.13) | copy-start | bytes 285700
  200.3 51.4 %all-gather.12.cloned.1.call-start = ((), (), s32[]{:S(2)}) async-start(), calls=%async_computation.7 | async-start | bytes 1966080 | tf_op jit(solution)/shard_map/all_gather | solution.py:40
  231.8 74.1 %reduce-scatter.6.cloned.1.call-start = ((), (), s32[]{:S(2)}) async-start(), calls=%async_computation.8 | async-start | bytes 1966080 | tf_op jit(solution)/shard_map/reduce_scatter | solution.py:70
  255.9 9.2 %copy-start.13 = (f32[1,1,256]{2,1,0:T(1,128)S(1)}, f32[1,1,256]{2,1,0:T(1,128)}, u32[]{:S(2)}) copy-start(f32[1,1,256]{2,1,0:T(1,128)} %get-tuple-element.90) | copy-start | bytes 3076
  257.8 5.9 %collective-permute-start.10 = (bf16[15,256]{1,0:T(8,128)(2,1)S(1)}, bf16[15,256]{1,0:T(8,128)(2,1)S(1)}, u32[]{:S(2)}, u32[]{:S(2)}) collective-permute-start(bf16[15,256]{1,0:T(8,128)(2,1)S(1)} %get-tuple-element.29), channel_id=1, source_target_pairs={{4,0},{8,4},{12,8},{16,12},{20,16},{24,20},{28,24},{5,1},{9,5},{13... | collective-permute-start | bytes 23048 | tf_op jit(solution)/shard_map/ppermute | solution.py:17
  259.1 5.9 %collective-permute-start.9 = (bf16[15,256]{1,0:T(8,128)(2,1)S(1)}, bf16[15,256]{1,0:T(8,128)(2,1)S(1)}, u32[]{:S(2)}, u32[]{:S(2)}) collective-permute-start(bf16[15,256]{1,0:T(8,128)(2,1)S(1)} %get-tuple-element.28), channel_id=1, source_target_pairs={{0,4},{4,8},{8,12},{12,16},{16,20},{20,24},{24,28},{1,5},{5,9},{9,... | collective-permute-start | bytes 23048 | tf_op jit(solution)/shard_map/ppermute | solution.py:16
  272.7 33.2 %copy-start = (bf16[384,512]{1,0:T(8,128)(2,1)S(1)}, bf16[384,512]{1,0:T(8,128)(2,1)}, u32[]{:S(2)}) copy-start(bf16[384,512]{1,0:T(8,128)(2,1)} %add_convert_fusion.2) | copy-start | bytes 1179652
  275.8 51.7 %all-gather.14.cloned.1.call-start = ((), (), s32[]{:S(2)}) async-start(), calls=%async_computation.9 | async-start | bytes 1966080 | tf_op jit(solution)/shard_map/all_gather | solution.py:40
  307.7 74.0 %reduce-scatter.8.cloned.1.call-start = ((), (), s32[]{:S(2)}) async-start(), calls=%async_computation.10 | async-start | bytes 1966080 | tf_op jit(solution)/shard_map/reduce_scatter | solution.py:70
  333.7 5.9 %collective-permute-start.12 = (bf16[15,256]{1,0:T(8,128)(2,1)S(1)}, bf16[15,256]{1,0:T(8,128)(2,1)S(1)}, u32[]{:S(2)}, u32[]{:S(2)}) collective-permute-start(bf16[15,256]{1,0:T(8,128)(2,1)S(1)} %get-tuple-element.27), channel_id=1, source_target_pairs={{4,0},{8,4},{12,8},{16,12},{20,16},{24,20},{28,24},{5,1},{9,5},{13... | collective-permute-start | bytes 23048 | tf_op jit(solution)/shard_map/ppermute | solution.py:17
  335.0 5.9 %collective-permute-start.11 = (bf16[15,256]{1,0:T(8,128)(2,1)S(1)}, bf16[15,256]{1,0:T(8,128)(2,1)S(1)}, u32[]{:S(2)}, u32[]{:S(2)}) collective-permute-start(bf16[15,256]{1,0:T(8,128)(2,1)S(1)} %get-tuple-element.26), channel_id=1, source_target_pairs={{0,4},{4,8},{8,12},{12,16},{16,20},{20,24},{24,28},{1,5},{5,9},{9,... | collective-permute-start | bytes 23048 | tf_op jit(solution)/shard_map/ppermute | solution.py:16
  348.5 33.3 %copy-start.1 = (bf16[384,512]{1,0:T(8,128)(2,1)S(1)}, bf16[384,512]{1,0:T(8,128)(2,1)}, u32[]{:S(2)}) copy-start(bf16[384,512]{1,0:T(8,128)(2,1)} %add_convert_fusion.1) | copy-start | bytes 1179652
  (15 other events, 110.1 us)
Sparse Core Ops, SparseCore 0:
  8.9 22.3 all-gather.5
  33.5 82.0 all-gather.9
  117.7 62.3 all-gather.7
  200.4 29.5 reduce-scatter.3
  231.9 19.6 all-gather.11
  275.9 29.9 reduce-scatter.5
  307.9 19.6 all-gather.13
  351.8 29.9 reduce-scatter.7
